TPU v7x, 32 devices: a whole 2x2x4 slice. The times are simulated.
32 devices in a mesh: sp: 8 (over z, y), tp: 4 (over x, core).
Axes of the slice: x: 2, y: 2, z: 4, core: 2. Of those that a mesh axis runs over, the one named last changes fastest.
Arguments:
- queries: bfloat16 [1536, 1024], P('sp', 'tp'), may hold values from -0.75 to 0.75
- key_vectors: bfloat16 [1536, 1024], P('sp', 'tp'), may hold values from -0.75 to 0.75
- values_in: bfloat16 [1536, 2048], P('sp', 'tp'), may hold values from -0.75 to 0.75
- log_decay: float32 [1536, 1024], P('sp', 'tp'), may hold values from -1 to 0
- mixed_heads: bfloat16 [1536, 2048], P('sp', 'tp'), may hold values from -6 to 6
- out_proj: bfloat16 [2048, 2048], P('tp'), may hold values from -0.125 to 0.125
- layer_input: bfloat16 [1536, 2048], P('sp'), may hold values from -6 to 6
- cotangent: bfloat16 [1536, 2048], P('sp'), may hold values from -6 to 6
- routes: int32 [1536, 2], P('sp'), may hold values from 0 to 15, all different within a row; in each aligned block of 192 rows (0 to 191, 192 to 383, ...) at most 48 rows name the same one
- route_weight: float32 [1536, 2], P('sp'), may hold values from 0.25 to 2
- gate_weight: bfloat16 [16, 2048, 1024], P('sp', None, 'tp'), may hold values from -0.125 to 0.125
- up_weight: bfloat16 [16, 2048, 1024], P('sp', None, 'tp'), may hold values from -0.125 to 0.125
- down_weight: bfloat16 [16, 1024, 2048], P('sp', 'tp'), may hold values from -0.1875 to 0.1875
Outputs:
- grad_gate: float32 [16, 2048, 1024], P('sp', None, 'tp')
- grad_up: float32 [16, 2048, 1024], P('sp', None, 'tp')
- grad_down: float32 [16, 1024, 2048], P('sp', 'tp')
- grad_proj: float32 [2048, 2048], P('sp', 'tp')
- grad_query: float32 [1536, 1024], P('sp', 'tp')
- grad_key: float32 [1536, 1024], P('sp', 'tp')
- grad_value: float32 [1536, 2048], P('sp', 'tp')
- grad_decay: float32 [1536, 1024], P('sp', 'tp')
Inputs may be any that keep to these rules, and one draw needn't show every extreme that they name: `routes`: in each aligned block of 192 tokens no expert is named by more than 48 pairs, and in some block one expert is named by exactly 48 pairs; the 2 experts of a token differ.
All inputs are finite; a program needn't handle non-finite values.
Results may differ from a plain program's by a relative error of at most 0.015.
Values may be sent and summed in bfloat16 or wider, within the bound.
A program may use at most 192 MiB of HBM per device.

v0:
```python
import functools

import jax
import jax.numpy as jnp
from jax import lax
from jax.experimental import pallas as pl
from jax.experimental.pallas import tpu as pltpu
from jax.sharding import PartitionSpec as P

DK = 128
DV = 256
VMEM = pltpu.VMEM
ANY = pl.ANY


def remote(source, target, send_sem, recv_sem, device):
    return pltpu.make_async_remote_copy(
        src_ref=source,
        dst_ref=target,
        send_sem=send_sem,
        recv_sem=recv_sem,
        device_id=device,
        device_id_type=pl.DeviceIdType.MESH,
    )


def greet(seq, tensor, s, tp_peers):
    barrier = pltpu.get_barrier_semaphore()
    for d in range(1, seq):
        pl.semaphore_signal(
            barrier,
            inc=1,
            device_id={"sp": lax.rem(s + d, seq)},
            device_id_type=pl.DeviceIdType.MESH,
        )
    for peer in tp_peers:
        pl.semaphore_signal(
            barrier, inc=1, device_id={"tp": peer}, device_id_type=pl.DeviceIdType.MESH
        )
    pl.semaphore_wait(barrier, seq - 1 + len(tp_peers))


def neighbours(tensor):
    t = lax.axis_index("tp")
    beside = t + 1 - 2 * lax.rem(t, 2)
    across = lax.rem(t + tensor // 2, tensor)
    return t, beside, across


class Relay:
    def __init__(self, seq, s, source, out, send_sem, recv_sem):
        self.half = seq // 2
        other = s + 1 - 2 * lax.rem(s, 2)

        def direct(j):
            to = lax.rem(s + 2 * j, seq)
            return remote(source(to), out.at[s], send_sem(j), recv_sem(j), {"sp": to})

        def onward(j):
            block = lax.rem(s - 2 * j + seq, seq)
            place = self.half + j
            held = out.at[block] if j else source(other)
            return remote(held, out.at[block], send_sem(place), recv_sem(place), {"sp": other})

        self.direct, self.onward = direct, onward

    def start(self):
        for j in range(1, self.half):
            self.direct(j).start()
        self.onward(0).start()

    def forward(self):
        for j in range(1, self.half):
            self.direct(j).wait_recv()
            self.onward(j).start()

    def finish(self):
        for j in range(self.half):
            if j:
                self.direct(j).wait_send()
            self.onward(j).wait()


def dispatch_kernel(
    seq,
    tensor,
    width,
    rows_ref,
    cot_ref,
    total_ref,
    state_ref,
    rows_out,
    cot_out,
    total_out,
    state_out,
    sp_send,
    sp_recv,
    tp_send,
    tp_recv,
    small_send,
    small_recv,
    own_sem,
):
    s = lax.axis_index("sp")
    t, beside, across = neighbours(tensor)
    ins, outs = (rows_ref, cot_ref), (rows_out, cot_out)
    greet(seq, tensor, s, (beside, across))

    def place(a, block, part):
        return outs[a].at[:, block, :, pl.ds(pl.multiple_of(part * width, width), width)]

    def spread(a, d):
        to = lax.rem(s + d, seq)
        return remote(
            ins[a].at[to], place(a, s, t), sp_send.at[a, d], sp_recv.at[a, d], {"sp": to}
        )

    def origin(d):
        return lax.rem(s - d + seq, seq)

    def forward(a, d, way):
        block = origin(d)
        part = across if way == 2 else t
        source = ins[a].at[s] if d == 0 and way != 2 else place(a, block, part)
        return remote(
            source,
            place(a, block, part),
            tp_send.at[way, a, d],
            tp_recv.at[way, a, d],
            {"tp": across if way == 1 else beside},
        )

    def small(d):
        to = lax.rem(s + d, seq)
        return remote(
            total_ref, total_out.at[s], small_send.at[0, d], small_recv.at[0, d], {"sp": to}
        )

    states = Relay(
        seq,
        s,
        lambda to: state_ref.at[jnp.where(to > s, 0, 1)],
        state_out,
        lambda i: small_send.at[1, i],
        lambda i: small_recv.at[1, i],
    )

    for d in range(1, seq):
        for a in range(2):
            spread(a, d).start()
    own = [
        pltpu.make_async_copy(ins[a].at[s], place(a, s, t), own_sem.at[a]) for a in range(2)
    ] + [
        pltpu.make_async_copy(total_ref, total_out.at[s], own_sem.at[2]),
        pltpu.make_async_copy(state_ref.at[0], state_out.at[s], own_sem.at[3]),
    ]
    for copy in own:
        copy.start()
    for a in range(2):
        forward(a, 0, 1).start()
        forward(a, 0, 0).start()
    for d in range(1, seq):
        small(d).start()
    states.start()
    lag = 2
    for d in range(1, seq + lag):
        if d < seq:
            for a in range(2):
                spread(a, d).wait_recv()
                forward(a, d, 1).start()
                forward(a, d, 0).start()
        if d >= lag:
            for a in range(2):
                forward(a, d - lag, 1).wait_recv()
                forward(a, d - lag, 2).start()
    states.forward()
    for d in range(seq):
        for a in range(2):
            if d:
                spread(a, d).wait_send()
            forward(a, d, 0).wait()
            forward(a, d, 1).wait_send()
            forward(a, d, 2).wait()
        if d:
            small(d).wait()
    states.finish()
    for copy in own:
        copy.wait()


def return_kernel(
    seq,
    tensor,
    width,
    part_ref,
    cot_ref,
    pick_ref,
    mixed_ref,
    token_out,
    mixed_out,
    arrived,
    summed,
    back,
    total,
    red_send,
    red_recv,
    sp_send,
    sp_recv,
    mix_send,
    mix_recv,
    tok_send,
    tok_recv,
    own_sem,
):
    s = lax.axis_index("sp")
    t, beside, across = neighbours(tensor)
    experts = part_ref.shape[0]
    greet(seq, tensor, s, tuple(lax.rem(t + u, tensor) for u in range(1, tensor)))

    def columns(part):
        return pl.ds(pl.multiple_of(part * width, width), width)

    def reduce(d, u):
        block = lax.rem(s + d, seq)
        to = lax.rem(t + u, tensor)
        return remote(
            part_ref.at[:, block, :, columns(to)],
            arrived.at[u - 1, d],
            red_send.at[u - 1, d],
            red_recv.at[u - 1, d],
            {"tp": to},
        )

    def give(d):
        to = lax.rem(s + d, seq)
        return remote(summed.at[d], back.at[d], sp_send.at[d], sp_recv.at[d], {"sp": to})

    mix = Relay(
        seq,
        s,
        lambda to: mixed_ref,
        mixed_out,
        lambda i: mix_send.at[i],
        lambda i: mix_recv.at[i],
    )

    def token(way):
        part = across if way == 2 else t
        return remote(
            token_out.at[part],
            token_out.at[part],
            tok_send.at[way],
            tok_recv.at[way],
            {"tp": across if way == 1 else beside},
        )

    order = list(range(1, seq)) + [0]
    for d in order:
        for u in range(1, tensor):
            reduce(d, u).start()
    own = pltpu.make_async_copy(mixed_ref, mixed_out.at[s], own_sem)
    own.start()
    mix.start()
    for d in order:
        block = lax.rem(s + d, seq)
        for u in range(1, tensor):
            reduce(d, u).wait_recv()
        for e in range(experts):
            value = part_ref[e, block, :, columns(t)].astype(jnp.float32)
            for u in range(1, tensor):
                value += arrived[u - 1, d, e].astype(jnp.float32)
            summed[d, e] = value.astype(jnp.bfloat16)
        if d:
            give(d).start()
    mix.forward()
    total[...] = cot_ref[...].astype(jnp.float32)
    for d in [0] + list(range(1, seq)):
        block = lax.rem(s - d + seq, seq)
        if d:
            give(d).wait_recv()
        held = back if d else summed
        term = total[...]
        for e in range(experts):
            term += jnp.dot(
                pick_ref[block, e], held[d, e], preferred_element_type=jnp.float32
            )
        total[...] = term
    token_out[t] = total[...].astype(jnp.bfloat16)
    token(1).start()
    token(0).start()
    token(1).wait_recv()
    token(2).start()
    for d in range(seq):
        for u in range(1, tensor):
            reduce(d, u).wait_send()
        if d:
            give(d).wait_send()
    mix.finish()
    own.wait()
    token(0).wait()
    token(1).wait_send()
    token(2).wait()


def exchange_kernel(
    seq, tensor, state_ref, token_ref, state_out, token_out, send_sem, recv_sem, own_sem
):
    s = lax.axis_index("sp")
    greet(seq, tensor, s, ())

    states = Relay(
        seq,
        s,
        lambda to: state_ref.at[jnp.where(to > s, 0, 1)],
        state_out,
        lambda i: send_sem.at[0, i],
        lambda i: recv_sem.at[0, i],
    )

    def copy(d):
        to = lax.rem(s + d, seq)
        return remote(
            token_ref.at[to], token_out.at[s], send_sem.at[1, d], recv_sem.at[1, d], {"sp": to}
        )

    own = (
        pltpu.make_async_copy(state_ref.at[0], state_out.at[s], own_sem.at[0]),
        pltpu.make_async_copy(token_ref.at[s], token_out.at[s], own_sem.at[1]),
    )
    states.start()
    for d in range(1, seq):
        copy(d).start()
    for piece in own:
        piece.start()
    states.forward()
    for d in range(1, seq):
        copy(d).wait()
    states.finish()
    for piece in own:
        piece.wait()


def call(kernel, outs, in_spaces, out_spaces, scratch, number):
    return pl.pallas_call(
        kernel,
        out_shape=outs,
        in_specs=[pl.BlockSpec(memory_space=space) for space in in_spaces],
        out_specs=[pl.BlockSpec(memory_space=space) for space in out_spaces],
        scratch_shapes=scratch,
        compiler_params=pltpu.CompilerParams(collective_id=number, has_side_effects=True),
    )


def running_sum(value):
    row = jnp.arange(value.shape[0], dtype=jnp.int32)
    mask = (row[:, None] >= row[None, :]).astype(jnp.float32)
    return jnp.tensordot(mask, value, 1, precision=lax.Precision.HIGHEST)


def tail_sum(value):
    row = jnp.arange(value.shape[0], dtype=jnp.int32)
    mask = (row[:, None] <= row[None, :]).astype(jnp.float32)
    return jnp.tensordot(mask, value, 1, precision=lax.Precision.HIGHEST)


def local_parts(query_f, key_f, grad_f, pair, decays):
    highest = lax.Precision.HIGH
    sigma = query_f.shape[2] ** (-0.5)
    length = query_f.shape[0]
    cum = running_sum(decays)
    total = cum[-1]
    middle = 0.5 * total
    rise = jnp.exp(cum - middle)
    fall = jnp.exp(middle - cum)
    position = jnp.arange(length, dtype=jnp.int32)
    lower = (position[:, None] >= position[None, :])[None]
    score_fwd = (
        jnp.where(
            lower, jnp.einsum("thc,shc->hts", query_f * rise, key_f * fall, precision=highest), 0.0
        )
        * sigma
    )
    score_bwd = (
        jnp.where(
            lower, 0.0, jnp.einsum("thc,shc->hts", query_f * fall, key_f * rise, precision=highest)
        )
        * sigma
    )
    pair_fwd = jnp.where(lower, pair, 0.0)
    pair_bwd = jnp.where(lower, 0.0, pair)
    query_fwd = sigma * rise * jnp.einsum("hts,shc->thc", pair_fwd, key_f * fall, precision=highest)
    query_bwd = sigma * fall * jnp.einsum("hts,shc->thc", pair_bwd, key_f * rise, precision=highest)
    key_fwd = sigma * fall * jnp.einsum("hts,thc->shc", pair_fwd, query_f * rise, precision=highest)
    key_bwd = sigma * rise * jnp.einsum("hts,thc->shc", pair_bwd, query_f * fall, precision=highest)
    value_grad = jnp.einsum("hts,thv->shv", score_fwd + score_bwd, grad_f, precision=highest)
    return (query_fwd, query_bwd, key_fwd, key_bwd, value_grad, cum, total)


def state_terms(query_f, key_f, value_f, grad_f, cum, total):
    highest = lax.Precision.HIGH
    head_part = jnp.exp(cum)
    tail = jnp.exp(total - cum)
    kv_fwd = jnp.einsum("shc,shv->hcv", key_f * tail, value_f, precision=highest)
    qo_bwd = jnp.einsum("thc,thv->hcv", query_f * tail, grad_f, precision=highest)
    qo_fwd = jnp.einsum("thc,thv->hcv", query_f * head_part, grad_f, precision=highest)
    kv_bwd = jnp.einsum("shc,shv->hcv", key_f * head_part, value_f, precision=highest)
    return (jnp.exp(total), kv_fwd, qo_bwd, qo_fwd, kv_bwd)


def carried(parts, states, query_f, key_f, value_f, grad_f):
    highest = lax.Precision.HIGH
    sigma = query_f.shape[2] ** (-0.5)
    query_fwd, query_bwd, key_fwd, key_bwd, value_grad, cum, total = parts
    kv_low, qo_low, qo_high, kv_high = states
    head_part = jnp.exp(cum)
    tail = jnp.exp(total - cum)
    query_fwd = query_fwd + sigma * head_part * jnp.einsum(
        "thv,hcv->thc", grad_f, kv_low, precision=highest
    )
    query_bwd = query_bwd + sigma * tail * jnp.einsum(
        "thv,hcv->thc", grad_f, kv_high, precision=highest
    )
    key_fwd = key_fwd + sigma * tail * jnp.einsum(
        "shv,hcv->shc", value_f, qo_high, precision=highest
    )
    key_bwd = key_bwd + sigma * head_part * jnp.einsum(
        "shv,hcv->shc", value_f, qo_low, precision=highest
    )
    value_grad = value_grad + sigma * (
        jnp.einsum("shc,hcv->shv", key_f * tail, qo_high, precision=highest)
        + jnp.einsum("shc,hcv->shv", key_f * head_part, qo_low, precision=highest)
    )
    grad_cum = query_f * (query_fwd - query_bwd) - key_f * (key_fwd - key_bwd)
    return (query_fwd + query_bwd, key_fwd + key_bwd, value_grad, grad_cum)


def body(
    queries,
    key_vectors,
    values_in,
    log_decay,
    mixed_heads,
    out_proj,
    layer_input,
    cotangent,
    routes,
    route_weight,
    gate_weight,
    up_weight,
    down_weight,
):
    tokens, top = routes.shape
    seq = lax.axis_size("sp")
    tensor = lax.axis_size("tp")
    s = lax.axis_index("sp")
    experts = gate_weight.shape[0]
    all_experts = experts * seq
    capacity = 2 * tokens * top // all_experts
    model = cotangent.shape[1]
    width = model // tensor
    column = lax.axis_index("tp") * width
    bf16, f32 = jnp.bfloat16, jnp.float32
    dma = pltpu.SemaphoreType.DMA

    heads = queries.shape[1] // DK
    query_f = queries.reshape(tokens, heads, DK).astype(f32)
    key_f = key_vectors.reshape(tokens, heads, DK).astype(f32)
    value_f = values_in.reshape(tokens, heads, DV).astype(f32)
    decays = log_decay.reshape(tokens, heads, DK)
    cum = running_sum(decays)
    total = cum[-1]
    head_part = jnp.exp(cum)
    tail = jnp.exp(total - cum)
    high = lax.Precision.HIGH
    kv_fwd = jnp.einsum("shc,shv->hcv", key_f * tail, value_f, precision=high)
    kv_bwd = jnp.einsum("shc,shv->hcv", key_f * head_part, value_f, precision=high)
    kv_send = jnp.stack([kv_fwd, kv_bwd]).astype(bf16)

    flat_route = routes.reshape(-1)
    onehot = flat_route[:, None] == jnp.arange(all_experts, dtype=jnp.int32)[None, :]
    pair_id = jnp.arange(tokens * top, dtype=jnp.int32)
    before = (pair_id[:, None] > pair_id[None, :]).astype(bf16)
    counts = jnp.dot(before, onehot.astype(bf16), preferred_element_type=f32)
    rank = jnp.sum(jnp.where(onehot, counts, 0.0), axis=1).astype(jnp.int32)
    slot = (flat_route * capacity + rank).reshape(tokens, top)
    slot_id = jnp.arange(all_experts * capacity, dtype=jnp.int32)
    match = slot_id[:, None, None] == slot[None, :, :]
    chosen = jnp.any(match, axis=2).astype(bf16)
    slot_weight = jnp.sum(jnp.where(match, route_weight[None], 0.0), axis=(1, 2))
    pick = (
        jnp.any(
            slot_id.reshape(seq, experts, 1, capacity, 1) == slot[None, None, :, None, :], axis=4
        )
    ).astype(bf16)
    own_input = lax.dynamic_slice_in_dim(layer_input, column, width, 1)
    own_cot = lax.dynamic_slice_in_dim(cotangent, column, width, 1)
    block_shape = (seq, experts, capacity, width)
    rows_send = jnp.dot(chosen, own_input, preferred_element_type=f32).astype(bf16)
    cot_send = (
        slot_weight[:, None] * jnp.dot(chosen, own_cot, preferred_element_type=f32)
    ).astype(bf16)

    expert_shape = jax.ShapeDtypeStruct((experts, seq, capacity, model), bf16)
    expert_rows, weighted, total_all, kv_all = call(
        functools.partial(dispatch_kernel, seq, tensor, width),
        (
            expert_shape,
            expert_shape,
            jax.ShapeDtypeStruct((seq, heads, DK), f32),
            jax.ShapeDtypeStruct((seq, heads, DK, DV), bf16),
        ),
        (VMEM, VMEM, VMEM, VMEM),
        (ANY, ANY, VMEM, VMEM),
        [
            dma((2, seq)),
            dma((2, seq)),
            dma((3, 2, seq)),
            dma((3, 2, seq)),
            dma((2, seq)),
            dma((2, seq)),
            dma((4,)),
        ],
        0,
    )(rows_send.reshape(block_shape), cot_send.reshape(block_shape), total, kv_send)
    expert_rows = expert_rows.reshape(experts, seq * capacity, model)
    weighted = weighted.reshape(experts, seq * capacity, model)

    pre_gate = jnp.einsum("erd,edf->erf", expert_rows, gate_weight, preferred_element_type=f32)
    pre_up = jnp.einsum("erd,edf->erf", expert_rows, up_weight, preferred_element_type=f32)
    d_act = jnp.einsum("erd,efd->erf", weighted, down_weight, preferred_element_type=f32)
    sigmoid_gate = jax.nn.sigmoid(pre_gate)
    silu_gate = pre_gate * sigmoid_gate
    act = (silu_gate * pre_up).astype(bf16)
    d_gate = (d_act * pre_up * sigmoid_gate * (1.0 + pre_gate * (1.0 - sigmoid_gate))).astype(bf16)
    d_up = (d_act * silu_gate).astype(bf16)
    partial_value = (
        jnp.einsum("erf,edf->erd", d_gate, gate_weight, preferred_element_type=f32)
        + jnp.einsum("erf,edf->erd", d_up, up_weight, preferred_element_type=f32)
    ).astype(bf16)
    grad_gate, grad_up, grad_down = (
        jnp.einsum("erd,erf->edf", expert_rows, d_gate, preferred_element_type=f32),
        jnp.einsum("erd,erf->edf", expert_rows, d_up, preferred_element_type=f32),
        jnp.einsum("erf,erd->efd", act, weighted, preferred_element_type=f32),
    )

    token_parts, mixed_all = call(
        functools.partial(return_kernel, seq, tensor, width),
        (
            jax.ShapeDtypeStruct((tensor, tokens, width), bf16),
            jax.ShapeDtypeStruct((seq,) + mixed_heads.shape, bf16),
        ),
        (VMEM, VMEM, VMEM, VMEM),
        (VMEM, ANY),
        [
            pltpu.VMEM((tensor - 1,) + block_shape, bf16),
            pltpu.VMEM(block_shape, bf16),
            pltpu.VMEM(block_shape, bf16),
            pltpu.VMEM((tokens, width), f32),
            dma((tensor - 1, seq)),
            dma((tensor - 1, seq)),
            dma((seq,)),
            dma((seq,)),
            dma((seq,)),
            dma((seq,)),
            dma((3,)),
            dma((3,)),
            dma,
        ],
        1,
    )(
        partial_value.reshape(experts, seq, capacity, model),
        own_cot,
        pick,
        mixed_heads,
    )
    token_grad = jnp.transpose(token_parts, (1, 0, 2)).reshape(tokens, model)
    head_grad = lax.dot_general(
        token_grad, out_proj, (((1,), (1,)), ((), ())), preferred_element_type=f32
    )
    grad_f = head_grad.reshape(tokens, heads, DV)
    qo_bwd = jnp.einsum("thc,thv->hcv", query_f * tail, grad_f, precision=high)
    qo_fwd = jnp.einsum("thc,thv->hcv", query_f * head_part, grad_f, precision=high)
    qo_send = jnp.stack([qo_bwd, qo_fwd]).astype(bf16)
    share = model // seq
    token_send = jnp.transpose(token_grad.reshape(tokens, seq, share), (1, 0, 2))
    qo_all, token_all = call(
        functools.partial(exchange_kernel, seq, tensor),
        (
            jax.ShapeDtypeStruct((seq, heads, DK, DV), bf16),
            jax.ShapeDtypeStruct((seq, tokens, share), bf16),
        ),
        (VMEM, VMEM),
        (VMEM, VMEM),
        [dma((2, seq)), dma((2, seq)), dma((2,))],
        2,
    )(qo_send, token_send)
    grad_proj = lax.dot_general(
        token_all, mixed_all, (((0, 1), (0, 1)), ((), ())), preferred_element_type=f32
    )

    pair = jnp.einsum("thv,shv->hts", grad_f, value_f, precision=high)
    parts = local_parts(query_f, key_f, grad_f, pair, decays)
    block = jnp.arange(seq, dtype=jnp.int32)
    low_span = ((block[None, :] > block[:, None]) & (block[None, :] < s)).astype(f32)
    high_span = ((block[None, :] < block[:, None]) & (block[None, :] > s)).astype(f32)

    def carry(span, mask):
        logs = jnp.sum(span[:, :, None, None] * total_all[None], axis=1)
        return jnp.where(mask[:, None, None], jnp.exp(logs), 0.0)[..., None]

    low_scale = carry(low_span, block < s)
    high_scale = carry(high_span, block > s)
    kv_low = jnp.sum(low_scale * kv_all.astype(f32), axis=0)
    kv_high = jnp.sum(high_scale * kv_all.astype(f32), axis=0)
    qo_low = jnp.sum(low_scale * qo_all.astype(f32), axis=0)
    qo_high = jnp.sum(high_scale * qo_all.astype(f32), axis=0)
    query_grad, key_grad, value_grad, grad_cum = carried(
        parts, (kv_low, qo_low, qo_high, kv_high), query_f, key_f, value_f, grad_f
    )
    decay_all = jnp.exp(total)[..., None]
    beyond = DK ** (-0.5) * jnp.sum(
        (decay_all * kv_low + kv_fwd) * qo_high + (decay_all * qo_low + qo_bwd) * kv_high, axis=2
    )
    grad_decay = tail_sum(grad_cum) + beyond[None]
    return (
        grad_gate,
        grad_up,
        grad_down,
        grad_proj,
        query_grad.reshape(tokens, heads * DK),
        key_grad.reshape(tokens, heads * DK),
        value_grad.reshape(tokens, heads * DV),
        grad_decay.reshape(tokens, heads * DK),
    )


def solution(mesh):
    return jax.shard_map(
        body,
        mesh=mesh,
        in_specs=(
            P("sp", "tp"),
            P("sp", "tp"),
            P("sp", "tp"),
            P("sp", "tp"),
            P("sp", "tp"),
            P("tp", None),
            P("sp", None),
            P("sp", None),
            P("sp", None),
            P("sp", None),
            P("sp", None, "tp"),
            P("sp", None, "tp"),
            P("sp", "tp", None),
        ),
        out_specs=(
            P("sp", None, "tp"),
            P("sp", None, "tp"),
            P("sp", "tp", None),
            P("sp", "tp"),
            P("sp", "tp"),
            P("sp", "tp"),
            P("sp", "tp"),
            P("sp", "tp"),
        ),
        check_vma=False,
    )
```

profile of v0, /device:TPU:0, one launch (start us, length us, event | category | flops | bytes accessed | tf_op | source)
XLA Modules:
  0.0 221.0 jit_solution(7162890047081067595)
XLA Ops:
  0.7 1.3 fusion.42
  2.0 1.0 convert_bitcast_fusion
  3.0 1.3 fusion.40
  4.4 0.4 fusion.23
  4.7 0.3 copy-done.13
  5.0 0.7 pad_maximum_fusion.state_ref
  5.8 0.9 constant_dynamic-slice_fusion.cot_ref
  6.7 0.1 copy.108
  6.8 0.1 eq.42
  7.0 0.2 fusion.25
  7.2 0.1 convert_element_type.75
  7.4 0.2 fusion.9
  7.6 0.2 select_reduce_fusion
  7.8 1.3 multiply_convert_fusion
  9.1 2.2 %convolution_convert_fusion = bf16[768,512]{1,0:T(8,128)(2,1)} fusion(pred[768,192]{0,1:T(8,128)(4,1)S(1)} %fusion.9, bf16[192,2048]{1,0:T(8,128)(2,1)} %param.19, s32[]{:T(128)S(6)} %select_n.42), kind=kOutput, calls=%fused_computation.11 | convolution fusion | flops 151388160 | bytes 1130500 | tf_op jit(solution)/shard_map/dot_general | solution.py:498
  11.4 62.3 %shard_map.188 = (bf16[2,8,48,2048]{3,2,1,0:T(8,128)(2,1)}, bf16[2,8,48,2048]{3,2,1,0:T(8,128)(2,1)}, f32[8,2,128]{2,1,0:T(2,128)}, bf16[8,2,128,256]{3,2,1,0:T(8,128)(2,1)}) custom-call(bf16[8,2,48,512]{3,2,1,0:T(8,128)(2,1)} %bitcast.192, bf16[8,2,48,512]{3,2,1,0:T(8,128)(2,1)} %bitcast.195, f32[2,128]{1,0:T(2,128)} %bitcast.200, ...), custom_call_target="tpu_custom_call" | custom-call | tf_op jit(solution)/shard_map/pallas_call | solution.py:504
  73.7 3.7 %fusion.87 = f32[2,384,256]{2,1,0:T(8,128)S(1)} fusion(bf16[2,384,2048]{2,1,0:T(8,128)(2,1)} %bitcast.180, bf16[2,2048,256]{2,1,0:T(8,128)(2,1)} %param.24), kind=kOutput, calls=%fused_computation.157 | convolution fusion | flops 805306368 | bytes 6029312 | tf_op jit(solution)/shard_map/erd,edf->erf/dot_general | solution.py:529
  77.5 1.0 fusion.88
  78.5 1.4 copy-done.7
  79.9 0.6 copy-done.27
  80.5 1.2 multiply_convert_fusion.2
  81.8 1.0 fusion.91
  82.8 0.8 copy-done.3
  83.7 2.7 %add_convert_fusion = bf16[2,384,2048]{2,1,0:T(8,128)(2,1)} fusion(f32[2,384,2048]{2,1,0:T(8,128)S(1)} %fusion.91, bf16[2,384,256]{2,1,0:T(8,128)(2,1)S(1)} %get-tuple-element.32, bf16[2,2048,256]{2,1,0:T(8,128)(2,1)S(1)} %copy-done.3), kind=kOutput, calls=%fused_computation | convolution fusion | flops 808452096 | bytes 11927552 | tf_op jit(solution)/shard_map/erf,edf->erd/dot_general | solution.py:538
  86.3 0.2 compare_reduce_fusion
  86.7 1.2 copy.120.pick_ref
  87.9 67.3 %shard_map.189 = (bf16[4,192,512]{2,1,0:T(8,128)(2,1)}, bf16[8,192,512]{2,1,0:T(8,128)(2,1)}) custom-call(bf16[2,8,48,2048]{3,2,1,0:T(8,128)(2,1)} %bitcast.184, bf16[192,512]{1,0:T(8,128)(2,1)} %copy-done.20, bf16[8,2,192,48]{3,2,1,0:T(8,128)(2,1)} %copy.120.pick_ref, bf16[192,512]{1,0:T(8,128)(2,1)} %mixed_ref.1), custom_call_target="tpu_custom_call" | custom-call | tf_op jit(solution)/shard_map/pallas_call | solution.py:546
  155.2 1.7 copy.121
  157.0 1.5 reshape.232
  158.4 2.7 %fusion.92 = f32[192,2,256]{2,0,1:T(8,128)S(1)} fusion(bf16[192,2048,1]{1,0,2:T(8,128)(2,1)} %reshape.232, bf16[2,256,2048]{2,1,0:T(8,128)(2,1)} %bitcast.194), kind=kOutput, calls=%fused_computation.162 | convolution fusion | flops 402653184 | bytes 3276800 | tf_op jit(solution)/shard_map/dot_general | solution.py:577
  161.1 0.4 fusion.32
  161.6 0.4 fusion.24
  162.1 0.7 pad_maximum_fusion.1.state_ref
  162.8 2.4 %reshape_reshape.3 = bf16[192,8,256]{2,1,0:T(8,128)(2,1)} reshape(bf16[192,4,512]{2,1,0:T(4,128)(2,1)} %copy-done.4) | data formatting | bytes 1572864 | tf_op jit(solution)/shard_map/reshape;reshape | solution.py:585
  165.1 2.2 copy.219
  167.3 30.2 %shard_map.190 = (bf16[8,2,128,256]{3,2,1,0:T(8,128)(2,1)}, bf16[8,192,256]{2,1,0:T(8,128)(2,1)}) custom-call(bf16[2,2,128,256]{3,2,1,0:T(8,128)(2,1)} %pad_maximum_fusion.1.state_ref, bf16[8,192,256]{2,1,0:T(8,128)(2,1)} %bitcast.193), custom_call_target="tpu_custom_call" | custom-call | tf_op jit(solution)/shard_map/pallas_call | solution.py:586
  197.6 0.1 multiply_reduce_fusion
  197.7 0.1 exponential_select_fusion
  197.8 0.1 exponential_select_fusion.1
  197.9 2.4 %fusion.1 = (f32[2,128,256]{2,1,0:T(8,128)S(1)}, f32[2,128,256]{2,1,0:T(8,128)S(1)}, f32[2,128,256]{2,1,0:T(8,128)S(1)}, f32[2,128,256]{2,1,0:T(8,128)S(1)}) fusion(bf16[8,2,128,256]{3,2,1,0:T(8,128)(2,1)} %get-tuple-element.22, f32[8,2,128]{2,1,0:T(2,128)S(1)} %exponential_select_fusion, f32[8,2,128]{2,1,0:T(2,128)S(1)} %exponential_select_fusion.1, ...), kind=kLoop, calls=%fused_computation.6 | loop fusion | flops 4980736 | bytes 3162112 | tf_op jit(solution)/shard_map/reduce_sum | solution.py:614
  200.3 0.2 add_reduce_fusion
  200.6 0.3 fusion.37
  200.9 0.6 fusion.13
  201.5 0.3 fusion.12
  201.8 0.6 fusion.16
  202.3 0.3 fusion.15
  202.6 0.3 fusion.19
  203.0 0.3 fusion.18
  203.3 0.3 fusion.22
  203.7 0.3 fusion.21
  204.0 0.3 fusion.10
  204.3 0.7 copy.220
  205.0 0.3 fusion.75
  205.3 0.4 convolution_select_fusion
  205.7 0.4 fusion.5
  206.1 0.6 fusion.93
  206.7 0.4 fusion.8
  207.1 0.8 copy.155
  207.9 0.7 copy_bitcast_fusion.2
  208.6 0.7 copy_bitcast_fusion.3
  209.3 1.4 convolution_bitcast_fusion
  210.7 3.3 %fusion.27 = f32[2,256,2048]{2,1,0:T(8,128)} fusion(bf16[2,384,2048]{2,1,0:T(8,128)(2,1)S(1)} %bitcast.191, f32[2,384,256]{2,1,0:T(8,128)S(1)} %copy-done.10, f32[2,384,256]{2,1,0:T(8,128)S(1)} %copy-done.12), kind=kOutput, calls=%fused_computation.59 | convolution fusion | flops 806486016 | bytes 8912896 | tf_op jit(solution)/shard_map/erf,erd->efd/dot_general | solution.py:543
  214.1 3.5 %fusion.90 = f32[2,2048,256]{2,1,0:T(8,128)} fusion(bf16[2,384,2048]{2,1,0:T(8,128)(2,1)S(1)} %bitcast.182, bf16[2,384,256]{2,1,0:T(8,128)(2,1)S(1)} %copy-done.18), kind=kOutput, calls=%fused_computation.160 | convolution fusion | flops 805306368 | bytes 7733248 | tf_op jit(solution)/shard_map/erd,erf->edf/dot_general | solution.py:542
  217.5 3.5 %fusion.89 = f32[2,2048,256]{2,1,0:T(8,128)} fusion(bf16[2,384,2048]{2,1,0:T(8,128)(2,1)S(1)} %bitcast.183, bf16[2,384,256]{2,1,0:T(8,128)(2,1)S(1)} %copy-done.16), kind=kOutput, calls=%fused_computation.159 | convolution fusion | flops 805306368 | bytes 7733248 | tf_op jit(solution)/shard_map/erd,erf->edf/dot_general | solution.py:541
  (68 shorter events, 0.4 us)
Async XLA Ops:
  0.6 76.8 %copy-start = (bf16[2,2048,256]{2,1,0:T(8,128)(2,1)S(1)}, bf16[2,2048,256]{2,1,0:T(8,128)(2,1)}, u32[]{:S(2)}) copy-start(bf16[2,2048,256]{2,1,0:T(8,128)(2,1)} %param.23) | copy-start | bytes 6291460
  0.6 3.7 %copy-start.5 = (bf16[192,512]{1,0:T(8,128)(2,1)S(1)}, bf16[192,512]{1,0:T(8,128)(2,1)}, u32[]{:S(2)}) copy-start(bf16[192,512]{1,0:T(8,128)(2,1)} %param.15) | copy-start | bytes 589828
  0.7 6.0 %copy-start.24 = (s32[192,2]{0,1:T(2,128)S(1)}, s32[192,2]{0,1:T(2,128)}, u32[]{:S(2)}) copy-start(s32[192,2]{0,1:T(2,128)} %param.21) | copy-start | bytes 4612
  2.0 5.6 %copy-start.22 = (f32[1,2,128]{2,0,1:T(1,128)}, f32[1,2,128]{2,0,1:T(1,128)S(1)}, u32[]{:S(2)}) copy-start(f32[1,2,128]{2,0,1:T(1,128)S(1)} %slice.5) | copy-start | bytes 3076
  2.0 5.6 %copy-start.26 = (f32[192,2]{0,1:T(2,128)S(1)}, f32[192,2]{0,1:T(2,128)}, u32[]{:S(2)}) copy-start(f32[192,2]{0,1:T(2,128)} %param.22) | copy-start | bytes 4612
  4.3 0.7 copy-start.13
  6.7 67.0 %copy-start.20 = (bf16[192,512]{1,0:T(8,128)(2,1)}, bf16[192,512]{1,0:T(8,128)(2,1)S(1)}, u32[]{:S(2)}) copy-start(bf16[192,512]{1,0:T(8,128)(2,1)S(1)} %constant_dynamic-slice_fusion.cot_ref) | copy-start | bytes 589828
  73.7 3.7 %copy-start.1 = (bf16[2,8,48,2048]{3,2,1,0:T(8,128)(2,1)S(1)}, bf16[2,8,48,2048]{3,2,1,0:T(8,128)(2,1)}, u32[]{:S(2)}) copy-start(bf16[2,8,48,2048]{3,2,1,0:T(8,128)(2,1)} %get-tuple-element.16) | copy-start | bytes 9437188
  77.4 1.1 copy-start.9
  77.4 2.5 %copy-start.7 = (bf16[2,8,48,2048]{3,2,1,0:T(8,128)(2,1)S(1)}, bf16[2,8,48,2048]{3,2,1,0:T(8,128)(2,1)}, u32[]{:S(2)}) copy-start(bf16[2,8,48,2048]{3,2,1,0:T(8,128)(2,1)} %get-tuple-element.17) | copy-start | bytes 9437188
  77.4 3.1 %copy-start.27 = (bf16[2,256,2048]{2,1,0:T(8,128)(2,1)S(1)}, bf16[2,256,2048]{2,1,0:T(8,128)(2,1)}, u32[]{:S(2)}) copy-start(bf16[2,256,2048]{2,1,0:T(8,128)(2,1)} %param.25) | copy-start | bytes 6291460
  78.5 3.3 %copy-start.11 = (f32[2,384,256]{2,1,0:T(8,128)}, f32[2,384,256]{2,1,0:T(8,128)S(1)}, u32[]{:S(2)}) copy-start(f32[2,384,256]{2,1,0:T(8,128)S(1)} %fusion.88) | copy-start | bytes 2359300
  81.8 1.1 copy-start.15
  81.8 1.1 copy-start.17
  81.8 1.9 copy-start.3
  156.9 1.5 copy-start.4
  156.9 4.2 %copy-start.23 = (f32[1,2,128]{2,0,1:T(1,128)S(1)}, f32[1,2,128]{2,0,1:T(1,128)}, u32[]{:S(2)}) copy-start(f32[1,2,128]{2,0,1:T(1,128)} %copy-done.22) | copy-start | bytes 3076
  162.8 34.7 %copy-start.25 = (f32[8,2,128]{2,1,0:T(2,128)S(1)}, f32[8,2,128]{2,1,0:T(2,128)}, u32[]{:S(2)}) copy-start(f32[8,2,128]{2,1,0:T(2,128)} %get-tuple-element.21) | copy-start | bytes 24580
  197.5 2.8 %copy-start.14 = (f32[2,128,256]{2,1,0:T(8,128)S(1)}, f32[2,128,256]{2,1,0:T(8,128)}, u32[]{:S(2)}) copy-start(f32[2,128,256]{2,1,0:T(8,128)} %copy-done.13) | copy-start | bytes 786436
  197.9 2.7 %copy-start.6 = (bf16[192,512]{1,0:T(8,128)(2,1)S(1)}, bf16[192,512]{1,0:T(8,128)(2,1)}, u32[]{:S(2)}) copy-start(bf16[192,512]{1,0:T(8,128)(2,1)} %param.15) | copy-start | bytes 589828
  206.1 3.2 %copy-start.21 = (bf16[8,192,256]{2,1,0:T(8,128)(2,1)S(1)}, bf16[8,192,256]{2,1,0:T(8,128)(2,1)}, u32[]{:S(2)}) copy-start(bf16[8,192,256]{2,1,0:T(8,128)(2,1)} %get-tuple-element.19) | copy-start | bytes 2359300
  206.7 2.6 %copy-start.19 = (bf16[8,192,512]{2,1,0:T(8,128)(2,1)S(1)}, bf16[8,192,512]{2,1,0:T(8,128)(2,1)}, u32[]{:S(2)}) copy-start(bf16[8,192,512]{2,1,0:T(8,128)(2,1)} %get-tuple-element.20) | copy-start | bytes 4718596
  207.1 3.6 %copy-start.12 = (f32[2,384,256]{2,1,0:T(8,128)S(1)}, f32[2,384,256]{2,1,0:T(8,128)}, u32[]{:S(2)}) copy-start(f32[2,384,256]{2,1,0:T(8,128)} %copy-done.11) | copy-start | bytes 2359300
  207.9 2.8 %copy-start.8 = (bf16[2,8,48,2048]{3,2,1,0:T(8,128)(2,1)S(1)}, bf16[2,8,48,2048]{3,2,1,0:T(8,128)(2,1)}, u32[]{:S(2)}) copy-start(bf16[2,8,48,2048]{3,2,1,0:T(8,128)(2,1)} %get-tuple-element.17) | copy-start | bytes 9437188
  207.9 2.8 %copy-start.10 = (f32[2,384,256]{2,1,0:T(8,128)S(1)}, f32[2,384,256]{2,1,0:T(8,128)}, u32[]{:S(2)}) copy-start(f32[2,384,256]{2,1,0:T(8,128)} %copy-done.9) | copy-start | bytes 2359300
  210.7 3.4 %copy-start.2 = (bf16[2,8,48,2048]{3,2,1,0:T(8,128)(2,1)S(1)}, bf16[2,8,48,2048]{3,2,1,0:T(8,128)(2,1)}, u32[]{:S(2)}) copy-start(bf16[2,8,48,2048]{3,2,1,0:T(8,128)(2,1)} %get-tuple-element.16) | copy-start | bytes 9437188
  210.7 3.4 %copy-start.18 = (bf16[2,384,256]{2,1,0:T(8,128)(2,1)S(1)}, bf16[2,384,256]{2,1,0:T(8,128)(2,1)}, u32[]{:S(2)}) copy-start(bf16[2,384,256]{2,1,0:T(8,128)(2,1)} %copy-done.17) | copy-start | bytes 1179652
  214.1 3.5 %copy-start.16 = (bf16[2,384,256]{2,1,0:T(8,128)(2,1)S(1)}, bf16[2,384,256]{2,1,0:T(8,128)(2,1)}, u32[]{:S(2)}) copy-start(bf16[2,384,256]{2,1,0:T(8,128)(2,1)} %copy-done.15) | copy-start | bytes 1179652
where the time goes:
time: 225 us; the launch traced here: 221 us
  Pallas kernels  160 us (71%)
  matrix products  37.3 us (17%)
  local copies, waits for them, and re-layouts  15.2 us (7%)
  other arithmetic  7.53 us (3%)
    pallas_call x1, Pallas kernels, body(): call(functools.partial(return_kernel, seq, tensor, width), (jax.ShapeDtyp...  67.3 us
    pallas_call x1, Pallas kernels, body(): call(functools.partial(dispatch_kernel, seq, tensor, width), (expert_shap...  62.3 us
    pallas_call x1, Pallas kernels, body(): call(functools.partial(exchange_kernel, seq, tensor), (jax.ShapeDtypeStru...  30.2 us
    another operation x2, local copies, waits for them, and re-layouts, body(): token_grad.reshape(tokens, seq, share)  4.53 us

commit v1 on v0

v1 whole, which is shorter than its diff:
```python
import functools

import jax
import jax.numpy as jnp
from jax import lax
from jax.experimental import pallas as pl
from jax.experimental.pallas import tpu as pltpu
from jax.sharding import PartitionSpec as P

DK = 128
DV = 256
VMEM = pltpu.VMEM
ANY = pl.ANY


def remote(source, target, send_sem, recv_sem, device):
    return pltpu.make_async_remote_copy(
        src_ref=source,
        dst_ref=target,
        send_sem=send_sem,
        recv_sem=recv_sem,
        device_id=device,
        device_id_type=pl.DeviceIdType.MESH,
    )


def greet(seq, tensor, s, tp_peers):
    barrier = pltpu.get_barrier_semaphore()
    for d in range(1, seq):
        pl.semaphore_signal(
            barrier,
            inc=1,
            device_id={"sp": lax.rem(s + d, seq)},
            device_id_type=pl.DeviceIdType.MESH,
        )
    for peer in tp_peers:
        pl.semaphore_signal(
            barrier, inc=1, device_id={"tp": peer}, device_id_type=pl.DeviceIdType.MESH
        )
    pl.semaphore_wait(barrier, seq - 1 + len(tp_peers))


def neighbours(tensor):
    t = lax.axis_index("tp")
    beside = t + 1 - 2 * lax.rem(t, 2)
    across = lax.rem(t + tensor // 2, tensor)
    return t, beside, across


class Chain:
    def __init__(self, seq, own, own_over, out, send_sem, recv_sem):
        s = lax.axis_index("sp")
        side = lax.rem(s, 2)
        line = lax.div(s, 2)
        other = s + 1 - 2 * side
        self.half = half = seq // 2

        def has(way, j):
            return line >= j if way == 0 else line + j < half

        def block(way, j):
            return s - 2 * j if way == 0 else s + 2 * j

        def relay(way, i):
            source = out.at[block(way, i)] if i else own(way)
            return remote(
                source, out.at[block(way, i)], send_sem.at[way, i], recv_sem.at[way, i],
                {"sp": s + 2 - 4 * way},
            )

        def landed(way, j):
            spot = out.at[block(way, j)]
            return remote(
                spot, spot, send_sem.at[way, j - 1], recv_sem.at[way, j - 1],
                {"sp": s - 2 + 4 * way},
            )

        def over(way, j):
            source = out.at[block(way, j)] if j else own_over
            return remote(
                source, out.at[block(way, j)], send_sem.at[2 + way, j], recv_sem.at[2 + way, j],
                {"sp": other},
            )

        self.has, self.relay, self.landed, self.over = has, relay, landed, over

    def start(self):
        for way in range(2):
            @pl.when(self.has(1 - way, 1))
            def _():
                self.relay(way, 0).start()
        self.over(0, 0).start()

    def step(self, j):
        for way in range(2):
            @pl.when(self.has(way, j))
            def _():
                self.landed(way, j).wait_recv()
                if j < self.half - 1:
                    @pl.when(self.has(1 - way, 1))
                    def _():
                        self.relay(way, j).start()
                self.over(way, j).start()

    def finish(self):
        for way in range(2):
            for j in range(self.half):
                if j < self.half - 1:
                    @pl.when(self.has(1 - way, 1) & self.has(way, j))
                    def _():
                        self.relay(way, j).wait_send()
                if j or way == 0:
                    @pl.when(self.has(way, j))
                    def _():
                        self.over(way, j).wait()


def halved(value):
    high = value.astype(jnp.bfloat16)
    return high, (value - high.astype(jnp.float32)).astype(jnp.bfloat16)


def outer(left, right):
    return lax.dot_general(
        left, right, (((0,), (0,)), ((), ())), preferred_element_type=jnp.float32
    )


def across_rows(left, right):
    return lax.dot_general(
        left, right, (((1,), (1,)), ((), ())), preferred_element_type=jnp.float32
    )


def whole_kernel(
    seq,
    tensor,
    width,
    input_ref,
    cot_ref,
    meta_ref,
    slot_ref,
    mixed_ref,
    query_ref,
    key_ref,
    value_ref,
    decay_ref,
    gate_in,
    up_in,
    down_in,
    proj_in,
    rows_out,
    cot_out,
    dgate_out,
    dup_out,
    act_out,
    mixed_out,
    total_out,
    kv_out,
    qo_out,
    token_out,
    head_out,
    cum_out,
    own_out,
    rows_all,
    cots_all,
    gate_ref,
    up_ref,
    down_ref,
    proj_ref,
    held,
    stage,
    notes,
    part,
    pair_in,
    cross_out,
    cross_in,
    summed,
    back,
    total,
    tokens_all,
    kv_own,
    qo_own,
    sums,
    z_send,
    z_recv,
    y_send,
    y_recv,
    tp_send,
    tp_recv,
    note_send,
    note_recv,
    pair_send,
    pair_recv,
    cross_send,
    cross_recv,
    give_send,
    give_recv,
    mix_send,
    mix_recv,
    kv_send,
    kv_recv,
    qo_send,
    qo_recv,
    tok_send,
    tok_recv,
    sum_send,
    sum_recv,
    sp_send,
    sp_recv,
    gather_send,
    gather_recv,
    load_sem,
    save_sem,
):
    s = lax.axis_index("sp")
    side, line = lax.rem(s, 2), lax.div(s, 2)
    other = s + 1 - 2 * side
    t, beside, across = neighbours(tensor)
    opposite = lax.rem(beside + tensor // 2, tensor)
    half = seq // 2
    bf16, f32 = jnp.bfloat16, jnp.float32
    experts, _, cap, model = rows_all.shape
    hidden = gate_ref.shape[2]
    tokens = input_ref.shape[0]
    heads = qo_out.shape[1]
    ins, outs = (input_ref, cot_ref), (rows_all, cots_all)
    loads = [
        pltpu.make_async_copy(source, target, load_sem.at[i])
        for i, (source, target) in enumerate(
            ((gate_in, gate_ref), (up_in, up_ref), (down_in, down_ref), (proj_in, proj_ref))
        )
    ]
    greet(seq, tensor, s, (beside, across))

    def columns(piece):
        return pl.ds(pl.multiple_of(piece * width, width), width)

    def place(a, block, piece):
        return outs[a].at[:, block, :, columns(piece)]

    labels = [(0, 0)] + [(way, j) for way in range(2) for j in range(1, half)]

    def number(label):
        way, j = label
        return j if way == 0 else (half - 1 + j if j else 0)

    def line_of(label):
        way, j = label
        return line - j if way == 0 else line + j

    def has(label):
        way, j = label
        return line >= j if way == 0 else line + j < half

    def ahead(way, j):
        return line + j < half if way == 0 else line >= j

    def stride(way):
        return 2 - 4 * way

    def relay(way, i, a):
        block = line_of((way, i))
        source = held.at[a, block] if i else ins[a].at[:, columns(t)]
        return remote(
            source, held.at[a, block], z_send.at[way, i, a], z_recv.at[way, i, a],
            {"sp": s + stride(way)},
        )

    def landed(way, j, a):
        spot = held.at[a, line_of((way, j))]
        return remote(
            spot, spot, z_send.at[way, j - 1, a], z_recv.at[way, j - 1, a],
            {"sp": s - stride(way)},
        )

    def note(way, j):
        return remote(
            meta_ref, notes.at[line], note_send.at[way, j], note_recv.at[way, j],
            {"sp": s + stride(way) * j},
        )

    def noted(way, j):
        spot = notes.at[line_of((way, j))]
        return remote(
            spot, spot, note_send.at[way, j], note_recv.at[way, j], {"sp": s - stride(way) * j}
        )

    def pass_on(label, a):
        k = number(label)
        return remote(
            stage.at[a, k], place(a, 2 * line_of(label) + side, t), y_send.at[a, k],
            y_recv.at[a, k], {"sp": other},
        )

    def passed(label, a):
        k = number(label)
        spot = place(a, 2 * line_of(label) + 1 - side, t)
        return remote(stage.at[a, k], spot, y_send.at[a, k], y_recv.at[a, k], {"sp": other})

    def share(way, label, mate, a):
        k = number(label)
        block = 2 * line_of(label) + (1 - side if mate else side)
        spot = place(a, block, across if way == 2 else t)
        return remote(
            spot, spot, tp_send.at[way, mate, a, k], tp_recv.at[way, mate, a, k],
            {"tp": across if way == 1 else beside},
        )

    def matching(label, group):
        table = notes[line_of(label)] if label[1] else meta_ref[...]
        row = lax.broadcasted_iota(jnp.int32, (experts * cap, tokens), 0)
        row = (row + group * (experts * cap)).astype(f32)
        first, second = table[0:1] == row, table[1:2] == row
        pick = jnp.where(first | second, 1.0, 0.0).astype(bf16)
        weight = jnp.where(first, table[2:3], 0.0) + jnp.where(second, table[3:4], 0.0)
        return pick, jnp.sum(weight, axis=1, keepdims=True)

    def rows_of(pick, weight, a, data):
        value = jnp.dot(pick, data, preferred_element_type=f32)
        value = value * weight if a else value
        return [value[e * cap : (e + 1) * cap].astype(bf16) for e in range(experts)]

    def select(label, a, mine):
        pick, weight = matching(label, s if mine else other)
        block = 2 * line_of(label) + side
        data = held[a, line_of(label)] if label[1] else ins[a][:, columns(t)]
        for e, piece in enumerate(rows_of(pick, weight, a, data)):
            if mine:
                outs[a][e, block, :, columns(t)] = piece
            else:
                stage[a, number(label), e] = piece

    def select_own(a):
        pick, weight = matching((0, 0), s)
        for piece in range(tensor):
            span = slice(piece * width, (piece + 1) * width)
            for e, rows in enumerate(rows_of(pick, weight, a, ins[a][:, span])):
                outs[a][e, s, :, span] = rows

    def z_item(j, a):
        for way in range(2):
            @pl.when(has((way, j)))
            def _():
                landed(way, j, a).wait_recv()
                if j < half - 1:
                    @pl.when(ahead(way, 1))
                    def _():
                        relay(way, j, a).start()
        for way in range(2):
            @pl.when(has((way, j)))
            def _():
                label = (way, j)
                if a == 0:
                    noted(way, j).wait_recv()
                select(label, a, False)
                pass_on(label, a).start()
                select(label, a, True)
                share(1, label, 0, a).start()
                share(0, label, 0, a).start()

    def y_item(j, a):
        for label in ((0, 0),) if j == 0 else ((0, j), (1, j)):
            @pl.when(has(label))
            def _():
                passed(label, a).wait_recv()
                share(1, label, 1, a).start()
                share(0, label, 1, a).start()

    def x_item(j, a):
        for label in ((0, 0),) if j == 0 else ((0, j), (1, j)):
            @pl.when(has(label))
            def _():
                for mate in range(2):
                    if j or mate:
                        share(1, label, mate, a).wait_recv()
                        share(2, label, mate, a).start()

    for way in range(2):
        for j in range(1, half):
            @pl.when(ahead(way, j))
            def _():
                note(way, j).start()
    for a in range(2):
        for way in range(2):
            @pl.when(ahead(way, 1))
            def _():
                relay(way, 0, a).start()
    for a in range(2):
        select((0, 0), a, False)
        pass_on((0, 0), a).start()
    for load in loads:
        load.start()
    for a in range(2):
        select_own(a)

    position = lax.broadcasted_iota(jnp.int32, (tokens, tokens), 0)
    lower = position >= lax.broadcasted_iota(jnp.int32, (tokens, tokens), 1)
    cum_out[...] = jnp.dot(
        lower.astype(f32), decay_ref[...], preferred_element_type=f32,
        precision=lax.Precision.HIGHEST,
    )

    def spans(h):
        return slice(h * DK, (h + 1) * DK), slice(h * DV, (h + 1) * DV)

    def faded(h, source):
        span, _ = spans(h)
        cum = cum_out[:, span]
        value = source[:, span].astype(f32)
        last = cum[tokens - 1 : tokens]
        return value * jnp.exp(last - cum), value * jnp.exp(cum), last

    def kv_terms(h):
        _, wide = spans(h)
        late, early, last = faded(h, key_ref)
        sums[h : h + 1] = last
        for i, value in enumerate((late, early)):
            high, low = halved(value)
            state = outer(high, value_ref[:, wide]) + outer(low, value_ref[:, wide])
            kv_own[i, h] = state.astype(bf16)
            if i == 0:
                own_out[0, h] = state

    for h in range(heads):
        kv_terms(h)

    mix = Chain(seq, lambda way: mixed_ref, mixed_ref, mixed_out, mix_send, mix_recv)
    kv = Chain(
        seq, lambda way: kv_own.at[way], kv_own.at[jnp.where(other > s, 0, 1)], kv_out,
        kv_send, kv_recv,
    )
    qo = Chain(
        seq, lambda way: qo_own.at[way], qo_own.at[jnp.where(other > s, 0, 1)], qo_out,
        qo_send, qo_recv,
    )

    def give_sum(d):
        to = lax.rem(s + d, seq)
        return remote(sums, total_out.at[s], sum_send.at[d], sum_recv.at[d], {"sp": to})

    items = [(j, a) for j in range(half) for a in range(2)]
    count = len(items)
    for n in range(2, count + 3):
        if n < count:
            z_item(*items[n])
        if n == count:
            for d in range(1, seq):
                give_sum(d).start()
            kv.start()
            mix.start()
        if n == 2:
            y_item(*items[0])
        if n - 1 < count:
            y_item(*items[n - 1])
        if n == 4:
            x_item(*items[0])
            x_item(*items[1])
        if 2 <= n - 3 < count:
            x_item(*items[n - 3])
    saves = [
        pltpu.make_async_copy(mixed_ref, mixed_out.at[s], save_sem.at[0]),
        pltpu.make_async_copy(rows_all, rows_out, save_sem.at[1]),
        pltpu.make_async_copy(cots_all, cot_out, save_sem.at[2]),
    ]
    saves[0].start()
    kv_out[s] = kv_own[0]
    total_out[s] = sums[...]
    kv.step(1)
    mix.step(1)
    for label in labels:
        @pl.when(has(label))
        def _():
            for a in range(2):
                for mate in range(2):
                    if label[1] or mate:
                        share(0, label, mate, a).wait_recv()
                        share(2, label, mate, a).wait_recv()
    saves[1].start()
    saves[2].start()
    for load in loads[:3]:
        load.wait()

    def forward_rows(e, blocks):
        shape = (len(blocks) * cap, model)
        span = slice(blocks[0], blocks[-1] + 1)
        rows = rows_all[e, span].reshape(shape)
        cots = cots_all[e, span].reshape(shape)
        gate = jnp.dot(rows, gate_ref[e], preferred_element_type=f32)
        up = jnp.dot(rows, up_ref[e], preferred_element_type=f32)
        down = across_rows(cots, down_ref[e])
        sigmoid = jax.nn.sigmoid(gate)
        silu = gate * sigmoid
        kept = (len(blocks), cap, hidden)
        act_out[e, span] = (silu * up).astype(bf16).reshape(kept)
        dgate_out[e, span] = (
            (down * up * sigmoid * (1.0 + gate * (1.0 - sigmoid))).astype(bf16).reshape(kept)
        )
        dup_out[e, span] = (down * silu).astype(bf16).reshape(kept)

    group = max(1, seq // 2) if cap % 16 == 0 else 1
    for first in range(0, seq, group):
        for e in range(experts):
            forward_rows(e, range(first, first + group))
    if half > 2:
        kv.step(2)
        mix.step(2)

    def partial(d):
        block = lax.rem(s + d, seq)
        for e in range(experts):
            for piece in range(tensor):
                span = slice(piece * width, (piece + 1) * width)
                value = across_rows(dgate_out[e, block], gate_ref[e, span])
                value += across_rows(dup_out[e, block], up_ref[e, span])
                part[e, block, :, span] = value.astype(bf16)

    def pair(d, h):
        block = lax.rem(s + d, seq)
        return remote(
            part.at[:, block, :, columns(opposite if h else beside)],
            pair_in.at[d, h],
            pair_send.at[d, h],
            pair_recv.at[d, h],
            {"tp": beside},
        )

    def cross(d):
        return remote(
            cross_out.at[d], cross_in.at[d], cross_send.at[d], cross_recv.at[d], {"tp": across}
        )

    def give(d):
        to = lax.rem(s + d, seq)
        return remote(summed.at[d], back.at[d], give_send.at[d], give_recv.at[d], {"sp": to})

    def cross_step(d):
        block = lax.rem(s + d, seq)
        pair(d, 1).wait_recv()
        for e in range(experts):
            value = part[e, block, :, columns(across)].astype(f32)
            value += pair_in[d, 1, e].astype(f32)
            cross_out[d, e] = value.astype(bf16)
        cross(d).start()

    def sum_step(d):
        block = lax.rem(s + d, seq)
        pair(d, 0).wait_recv()
        cross(d).wait_recv()
        for e in range(experts):
            value = part[e, block, :, columns(t)].astype(f32)
            value += pair_in[d, 0, e].astype(f32)
            value += cross_in[d, e].astype(f32)
            summed[d, e] = value.astype(bf16)
        if d:
            give(d).start()

    order = sorted(range(seq), key=lambda d: (d == 0, -min(d, seq - d), d))
    for i in range(seq + 3):
        if i < seq:
            partial(order[i])
            for h in (1, 0):
                pair(order[i], h).start()
        if 1 <= i <= seq:
            cross_step(order[i - 1])
        if i >= 3:
            sum_step(order[i - 3])
    for j in range(3, half):
        kv.step(j)
        mix.step(j)

    row = lax.broadcasted_iota(jnp.int32, (tokens, cap), 1)
    total[...] = cot_ref[:, columns(t)].astype(f32)
    for d in [0] + order[:-1]:
        block = lax.rem(s - d + seq, seq)
        if d:
            give(d).wait_recv()
        source = back if d else summed
        term = total[...]
        for e in range(experts):
            wanted = row + (block * experts + e) * cap
            match = (slot_ref[:, 0:1] == wanted) | (slot_ref[:, 1:2] == wanted)
            pick = jnp.where(match, 1.0, 0.0).astype(bf16)
            term += jnp.dot(pick, source[d, e], preferred_element_type=f32)
        total[...] = term
    tokens_all[:, columns(t)] = total[...].astype(bf16)

    def token(way):
        spot = tokens_all.at[:, columns(across if way == 2 else t)]
        return remote(
            spot, spot, tok_send.at[way], tok_recv.at[way],
            {"tp": across if way == 1 else beside},
        )

    token(1).start()
    token(0).start()
    loads[3].wait()
    token(1).wait_recv()
    token(2).start()
    token(0).wait_recv()
    token(2).wait_recv()

    share_span = token_out.shape[2]
    pack = share_span * seq // model
    quarter_rows = tokens // tensor

    def share_columns(to):
        return pl.ds(pl.multiple_of(lax.div(to, pack) * share_span, share_span), share_span)

    def quarter(piece):
        return pl.ds(pl.multiple_of(piece * quarter_rows, quarter_rows), quarter_rows)

    def spread(d):
        to = lax.rem(s + d, seq)
        return remote(
            tokens_all.at[quarter(t), share_columns(to)],
            token_out.at[s, quarter(t)],
            sp_send.at[d],
            sp_recv.at[d],
            {"sp": to},
        )

    def gather(d, way):
        spot = token_out.at[lax.rem(s - d + seq, seq), quarter(across if way == 2 else t)]
        return remote(
            spot, spot, gather_send.at[way, d], gather_recv.at[way, d],
            {"tp": across if way == 1 else beside},
        )

    for d in range(1, seq):
        spread(d).start()
    for h in range(heads):
        _, wide = spans(h)
        grad = across_rows(tokens_all[...], proj_ref[wide])
        head_out[:, wide] = grad
        grad_high, grad_low = halved(grad)
        late, early, _ = faded(h, query_ref)
        for i, value in enumerate((late, early)):
            high, low = halved(value)
            state = outer(high, grad_high) + outer(low, grad_high) + outer(high, grad_low)
            qo_own[i, h] = state.astype(bf16)
            if i == 0:
                own_out[1, h] = state
    qo.start()
    qo_out[s] = qo_own[0]
    token_out[s] = tokens_all[:, share_columns(s)]
    for j in range(1, half):
        qo.step(j)
    for d in range(1, seq):
        spread(d).wait_recv()
        gather(d, 1).start()
        gather(d, 0).start()
    for d in range(1, seq):
        gather(d, 1).wait_recv()
        gather(d, 2).start()

    for label in labels:
        @pl.when(has(label))
        def _():
            way, j = label
            for a in range(2):
                if j < half - 1:
                    for onto in range(2) if j == 0 else (way,):
                        @pl.when(ahead(onto, 1))
                        def _():
                            relay(onto, j, a).wait_send()
                pass_on(label, a).wait_send()
                for mate in range(2):
                    if j or mate:
                        for onto in range(3):
                            share(onto, label, mate, a).wait_send()
    for way in range(2):
        for j in range(1, half):
            @pl.when(ahead(way, j))
            def _():
                note(way, j).wait_send()
    for d in range(seq):
        for h in range(2):
            pair(d, h).wait_send()
        cross(d).wait_send()
        if d:
            give(d).wait_send()
            give_sum(d).wait()
            spread(d).wait_send()
            gather(d, 0).wait()
            gather(d, 1).wait_send()
            gather(d, 2).wait()
    for way in range(3):
        token(way).wait_send()
    for save in saves:
        save.wait()
    mix.finish()
    kv.finish()
    qo.finish()


def call(kernel, outs, in_spaces, out_spaces, scratch, number):
    return pl.pallas_call(
        kernel,
        out_shape=outs,
        in_specs=[pl.BlockSpec(memory_space=space) for space in in_spaces],
        out_specs=[pl.BlockSpec(memory_space=space) for space in out_spaces],
        scratch_shapes=scratch,
        compiler_params=pltpu.CompilerParams(collective_id=number, has_side_effects=True),
    )


def tail_sum(value):
    row = jnp.arange(value.shape[0], dtype=jnp.int32)
    mask = (row[:, None] <= row[None, :]).astype(jnp.float32)
    return jnp.tensordot(mask, value, 1, precision=lax.Precision.HIGHEST)


def local_parts(query_f, key_f, grad_f, pair, cum):
    highest = lax.Precision.HIGH
    sigma = query_f.shape[2] ** (-0.5)
    length = query_f.shape[0]
    total = cum[-1]
    middle = 0.5 * total
    rise = jnp.exp(cum - middle)
    fall = jnp.exp(middle - cum)
    position = jnp.arange(length, dtype=jnp.int32)
    lower = (position[:, None] >= position[None, :])[None]
    score_fwd = (
        jnp.where(
            lower, jnp.einsum("thc,shc->hts", query_f * rise, key_f * fall, precision=highest), 0.0
        )
        * sigma
    )
    score_bwd = (
        jnp.where(
            lower, 0.0, jnp.einsum("thc,shc->hts", query_f * fall, key_f * rise, precision=highest)
        )
        * sigma
    )
    pair_fwd = jnp.where(lower, pair, 0.0)
    pair_bwd = jnp.where(lower, 0.0, pair)
    query_fwd = sigma * rise * jnp.einsum("hts,shc->thc", pair_fwd, key_f * fall, precision=highest)
    query_bwd = sigma * fall * jnp.einsum("hts,shc->thc", pair_bwd, key_f * rise, precision=highest)
    key_fwd = sigma * fall * jnp.einsum("hts,thc->shc", pair_fwd, query_f * rise, precision=highest)
    key_bwd = sigma * rise * jnp.einsum("hts,thc->shc", pair_bwd, query_f * fall, precision=highest)
    value_grad = jnp.einsum("hts,thv->shv", score_fwd + score_bwd, grad_f, precision=highest)
    return (query_fwd, query_bwd, key_fwd, key_bwd, value_grad, cum, total)


def carried(parts, states, query_f, key_f, value_f, grad_f):
    highest = lax.Precision.HIGH
    sigma = query_f.shape[2] ** (-0.5)
    query_fwd, query_bwd, key_fwd, key_bwd, value_grad, cum, total = parts
    kv_low, qo_low, qo_high, kv_high = states
    head_part = jnp.exp(cum)
    tail = jnp.exp(total - cum)
    query_fwd = query_fwd + sigma * head_part * jnp.einsum(
        "thv,hcv->thc", grad_f, kv_low, precision=highest
    )
    query_bwd = query_bwd + sigma * tail * jnp.einsum(
        "thv,hcv->thc", grad_f, kv_high, precision=highest
    )
    key_fwd = key_fwd + sigma * tail * jnp.einsum(
        "shv,hcv->shc", value_f, qo_high, precision=highest
    )
    key_bwd = key_bwd + sigma * head_part * jnp.einsum(
        "shv,hcv->shc", value_f, qo_low, precision=highest
    )
    value_grad = value_grad + sigma * (
        jnp.einsum("shc,hcv->shv", key_f * tail, qo_high, precision=highest)
        + jnp.einsum("shc,hcv->shv", key_f * head_part, qo_low, precision=highest)
    )
    grad_cum = query_f * (query_fwd - query_bwd) - key_f * (key_fwd - key_bwd)
    return (query_fwd + query_bwd, key_fwd + key_bwd, value_grad, grad_cum)


def body(
    queries,
    key_vectors,
    values_in,
    log_decay,
    mixed_heads,
    out_proj,
    layer_input,
    cotangent,
    routes,
    route_weight,
    gate_weight,
    up_weight,
    down_weight,
):
    tokens, top = routes.shape
    seq = lax.axis_size("sp")
    tensor = lax.axis_size("tp")
    s = lax.axis_index("sp")
    experts, _, hidden = gate_weight.shape
    all_experts = experts * seq
    capacity = 2 * tokens * top // all_experts
    model = cotangent.shape[1]
    width = model // tensor
    half = seq // 2
    bf16, f32 = jnp.bfloat16, jnp.float32
    dma = pltpu.SemaphoreType.DMA

    heads = queries.shape[1] // DK
    high = lax.Precision.HIGH

    flat_route = routes.reshape(-1)
    onehot = flat_route[:, None] == jnp.arange(all_experts, dtype=jnp.int32)[None, :]
    pair_id = jnp.arange(tokens * top, dtype=jnp.int32)
    before = (pair_id[:, None] > pair_id[None, :]).astype(bf16)
    counts = jnp.dot(before, onehot.astype(bf16), preferred_element_type=f32)
    rank = jnp.sum(jnp.where(onehot, counts, 0.0), axis=1).astype(jnp.int32)
    slot = (flat_route * capacity + rank).reshape(tokens, top)
    lines = jnp.concatenate([slot.astype(f32).T, route_weight.T], axis=0)
    meta = jnp.pad(lines, ((0, 8 - 2 * top), (0, 0)))

    share = model // seq
    pack = max(1, 128 // share)
    rows_shape = (experts, seq, capacity, model)
    block_shape = (seq, experts, capacity, width)
    hidden_shape = (experts, seq, capacity, hidden)
    state_shape = (seq, heads, DK, DV)
    labels = 2 * half - 1

    def struct(shape, dtype):
        return jax.ShapeDtypeStruct(shape, dtype)

    def sems(*shape):
        return [dma(shape), dma(shape)]

    (
        expert_rows,
        weighted,
        d_gate,
        d_up,
        act,
        mixed_all,
        total_all,
        kv_all,
        qo_all,
        token_all,
        head_grad,
        cum_flat,
        own_states,
    ) = call(
        functools.partial(whole_kernel, seq, tensor, width),
        (
            struct(rows_shape, bf16),
            struct(rows_shape, bf16),
            struct(hidden_shape, bf16),
            struct(hidden_shape, bf16),
            struct(hidden_shape, bf16),
            struct((seq,) + mixed_heads.shape, bf16),
            struct((seq, heads, DK), f32),
            struct(state_shape, bf16),
            struct(state_shape, bf16),
            struct((seq, tokens, share * pack), bf16),
            struct((tokens, heads * DV), f32),
            struct((tokens, heads * DK), f32),
            struct((2, heads, DK, DV), f32),
        ),
        (VMEM,) * 9 + (ANY,) * 4,
        (ANY, ANY, VMEM, VMEM, VMEM, ANY) + (VMEM,) * 7,
        [
            pltpu.VMEM(rows_shape, bf16),
            pltpu.VMEM(rows_shape, bf16),
            pltpu.VMEM(gate_weight.shape, bf16),
            pltpu.VMEM(up_weight.shape, bf16),
            pltpu.VMEM(down_weight.shape, bf16),
            pltpu.VMEM(out_proj.shape, bf16),
            pltpu.VMEM((2, half, tokens, width), bf16),
            pltpu.VMEM((2, labels, experts, capacity, width), bf16),
            pltpu.VMEM((half,) + meta.shape, f32),
            pltpu.VMEM(rows_shape, bf16),
            pltpu.VMEM((seq, 2, experts, capacity, width), bf16),
            pltpu.VMEM(block_shape, bf16),
            pltpu.VMEM(block_shape, bf16),
            pltpu.VMEM(block_shape, bf16),
            pltpu.VMEM(block_shape, bf16),
            pltpu.VMEM((tokens, width), f32),
            pltpu.VMEM((tokens, model), bf16),
            pltpu.VMEM((2, heads, DK, DV), bf16),
            pltpu.VMEM((2, heads, DK, DV), bf16),
            pltpu.VMEM((heads, DK), f32),
            *sems(2, half, 2),
            *sems(2, labels),
            *sems(3, 2, 2, labels),
            *sems(2, half),
            *sems(seq, 2),
            *sems(seq),
            *sems(seq),
            *sems(4, half),
            *sems(4, half),
            *sems(4, half),
            *sems(3),
            *sems(seq),
            *sems(seq),
            *sems(3, seq),
            dma((4,)),
            dma((3,)),
        ],
        0,
    )(
        layer_input,
        cotangent,
        meta,
        slot,
        mixed_heads,
        queries,
        key_vectors,
        values_in,
        log_decay,
        gate_weight,
        up_weight,
        down_weight,
        out_proj,
    )
    flat = (experts, seq * capacity)
    expert_rows, weighted = expert_rows.reshape(flat + (model,)), weighted.reshape(flat + (model,))
    d_gate, d_up, act = (value.reshape(flat + (hidden,)) for value in (d_gate, d_up, act))
    if pack > 1:
        token_all = lax.dynamic_slice_in_dim(token_all, lax.rem(s, pack) * share, share, 2)
    grad_gate, grad_up, grad_down = (
        jnp.einsum("erd,erf->edf", expert_rows, d_gate, preferred_element_type=f32),
        jnp.einsum("erd,erf->edf", expert_rows, d_up, preferred_element_type=f32),
        jnp.einsum("erf,erd->efd", act, weighted, preferred_element_type=f32),
    )
    grad_proj = lax.dot_general(
        token_all, mixed_all, (((0, 1), (0, 1)), ((), ())), preferred_element_type=f32
    )

    query_f = queries.reshape(tokens, heads, DK).astype(f32)
    key_f = key_vectors.reshape(tokens, heads, DK).astype(f32)
    value_f = values_in.reshape(tokens, heads, DV).astype(f32)
    grad_f = head_grad.reshape(tokens, heads, DV)
    cum = cum_flat.reshape(tokens, heads, DK)
    total = cum[-1]
    kv_fwd, qo_bwd = own_states[0], own_states[1]
    pair = jnp.einsum("thv,shv->hts", grad_f, value_f, precision=high)
    parts = local_parts(query_f, key_f, grad_f, pair, cum)
    block = jnp.arange(seq, dtype=jnp.int32)
    low_span = ((block[None, :] > block[:, None]) & (block[None, :] < s)).astype(f32)
    high_span = ((block[None, :] < block[:, None]) & (block[None, :] > s)).astype(f32)

    def carry(span, mask):
        logs = jnp.sum(span[:, :, None, None] * total_all[None], axis=1)
        return jnp.where(mask[:, None, None], jnp.exp(logs), 0.0)[..., None]

    low_scale = carry(low_span, block < s)
    high_scale = carry(high_span, block > s)
    kv_low = jnp.sum(low_scale * kv_all.astype(f32), axis=0)
    kv_high = jnp.sum(high_scale * kv_all.astype(f32), axis=0)
    qo_low = jnp.sum(low_scale * qo_all.astype(f32), axis=0)
    qo_high = jnp.sum(high_scale * qo_all.astype(f32), axis=0)
    query_grad, key_grad, value_grad, grad_cum = carried(
        parts, (kv_low, qo_low, qo_high, kv_high), query_f, key_f, value_f, grad_f
    )
    decay_all = jnp.exp(total)[..., None]
    beyond = DK ** (-0.5) * jnp.sum(
        (decay_all * kv_low + kv_fwd) * qo_high + (decay_all * qo_low + qo_bwd) * kv_high, axis=2
    )
    grad_decay = tail_sum(grad_cum) + beyond[None]
    return (
        grad_gate,
        grad_up,
        grad_down,
        grad_proj,
        query_grad.reshape(tokens, heads * DK),
        key_grad.reshape(tokens, heads * DK),
        value_grad.reshape(tokens, heads * DV),
        grad_decay.reshape(tokens, heads * DK),
    )


def solution(mesh):
    return jax.shard_map(
        body,
        mesh=mesh,
        in_specs=(
            P("sp", "tp"),
            P("sp", "tp"),
            P("sp", "tp"),
            P("sp", "tp"),
            P("sp", "tp"),
            P("tp", None),
            P("sp", None),
            P("sp", None),
            P("sp", None),
            P("sp", None),
            P("sp", None, "tp"),
            P("sp", None, "tp"),
            P("sp", "tp", None),
        ),
        out_specs=(
            P("sp", None, "tp"),
            P("sp", None, "tp"),
            P("sp", "tp", None),
            P("sp", "tp"),
            P("sp", "tp"),
            P("sp", "tp"),
            P("sp", "tp"),
            P("sp", "tp"),
        ),
        check_vma=False,
    )
```

time: 225 us -> 150 us (0.67); the launches traced: 221 us -> 149 us
  Pallas kernels: 160 us -> 119 us
  matrix products: 37.3 us -> 17.5 us
  local copies, waits for them, and re-layouts: 15.2 us -> 4.29 us
    pallas_call x3 -> x1, Pallas kernels: 160 us -> 119 us  [body(): call(functools.partial(whole_kernel, seq, tensor, width), (struct(rows_sh...]
    dot_general x13 -> x0, matrix products: 19.7 us -> none  [the longest x1 3.66 us: body(): jnp.einsum('erd,edf->erf', expert_rows, up_weight, preferred_element_type...]
    another operation x2 -> x0, local copies, waits for them, and re-layouts: 4.53 us -> none  [body(): token_grad.reshape(tokens, seq, share)]
    unnamed x57 -> x23, local copies, waits for them, and re-layouts: 3.4 us -> 0.84 us
where the time goes in v1:
time: 150 us; the launch traced here: 149 us
  Pallas kernels  119 us (79%)
  matrix products  17.5 us (12%)
  other arithmetic  7.94 us (5%)
  local copies, waits for them, and re-layouts  4.29 us (3%)
    pallas_call x1, Pallas kernels, body(): call(functools.partial(whole_kernel, seq, tensor, width), (struct(rows_sh...  119 us
    dot_general x1, matrix products, body(): jnp.einsum('erd,erf->edf', expert_rows, d_gate, preferred_element_type=f32)  3.48 us
    dot_general x1, matrix products, body(): jnp.einsum('erd,erf->edf', expert_rows, d_up, preferred_element_type=f32)  3.48 us
    dot_general x1, matrix products, body(): jnp.einsum('erf,erd->efd', act, weighted, preferred_element_type=f32)  3.31 us

profile of v1, /device:TPU:0, one launch (start us, length us, event | category | flops | bytes accessed | tf_op | source)
XLA Modules:
  0.0 149.4 jit_solution(18296492141827966423)
XLA Ops:
  0.6 0.7 broadcast_multiply_fusion
  1.4 0.1 copy.144
  1.5 0.8 copy.143
  2.3 0.1 eq.15
  2.5 0.2 fusion.22
  2.7 0.1 convert_element_type.51
  2.8 0.7 convert_bitcast_fusion.2
  3.5 0.1 copy.145
  3.6 1.3 select_maximum_fusion.meta_ref
  4.9 1.0 convert_bitcast_fusion
  5.8 118.8 %shard_map.188 = (bf16[2,8,48,2048]{3,2,1,0:T(8,128)(2,1)}, bf16[2,8,48,2048]{3,2,1,0:T(8,128)(2,1)}, bf16[2,8,48,256]{3,2,1,0:T(8,128)(2,1)}, bf16[2,8,48,256]{...) custom-call(bf16[192,2048]{1,0:T(8,128)(2,1)} %input_ref.1, ...), custom_call_target="tpu_custom_call" | custom-call | tf_op jit(solution)/shard_map/pallas_call | solution.py:842
  124.6 0.0 copy-start.7
  124.6 0.0 copy-start.2
  124.6 0.0 copy-start.4
  124.6 0.0 copy-start
  124.6 0.8 slice.11
  125.5 0.7 copy.155
  126.2 0.3 multiply_reduce_fusion
  126.5 0.1 exponential_select_fusion
  126.6 0.1 exponential_select_fusion.1
  126.7 2.2 %fusion.1 = (f32[2,128,256]{2,1,0:T(8,128)S(1)}, f32[2,128,256]{2,1,0:T(8,128)S(1)}, f32[2,128,256]{2,1,0:T(8,128)S(1)}, f32[2,128,256]{2,1,0:T(8,128)S(1)}) fusion(bf16[8,2,128,256]{3,2,1,0:T(8,128)(2,1)} %get-tuple-element.31, f32[8,2,128]{2,1,0:T(2,128)S(1)} %exponential_select_fusion, f32[8,2,128]{2,1,0:T(2,128)S(1)} %exponential_select_fusion.1, ...), kind=kLoop, calls=%fused_computation.5 | loop fusion | flops 4980736 | bytes 3162112 | tf_op jit(solution)/shard_map/reduce_sum | solution.py:949
  128.8 0.0 copy-done.7
  128.8 0.2 fusion.39
  129.1 0.0 copy-done.2
  129.1 0.0 copy-done.4
  129.1 0.3 fusion.27
  129.4 0.0 copy-done
  129.4 0.6 fusion.15
  130.0 0.3 fusion.14
  130.3 0.3 fusion.46
  130.6 0.6 fusion.12
  131.2 0.3 fusion.11
  131.4 0.7 copy_bitcast_fusion.1
  132.1 0.3 fusion.18
  132.5 0.3 fusion.17
  132.8 0.3 fusion.21
  133.2 0.3 fusion.20
  133.5 0.3 fusion.9
  133.8 0.7 copy_bitcast_fusion.2
  134.5 0.7 copy.290
  135.2 0.0 copy-start.5
  135.2 0.0 copy-start.6
  135.2 0.4 convolution_select_fusion
  135.6 0.4 fusion.5
  136.0 0.0 copy-start.1
  136.0 0.0 copy-start.10
  136.0 0.6 fusion.23
  136.6 0.4 fusion.8
  137.0 0.8 copy.189
  137.7 0.0 copy-done.5
  137.7 0.0 copy-done.6
  137.8 1.4 convolution_bitcast_fusion
  139.1 0.0 copy-done.1
  139.1 0.0 copy-done.10
  139.1 0.0 copy-start.9
  139.1 3.5 %fusion.94 = f32[2,2048,256]{2,1,0:T(8,128)} fusion(bf16[2,384,2048]{2,1,0:T(8,128)(2,1)S(1)} %bitcast.242, bf16[2,384,256]{2,1,0:T(8,128)(2,1)S(1)} %bitcast.255), kind=kOutput, calls=%fused_computation.148 | convolution fusion | flops 805306368 | bytes 7733248 | tf_op jit(solution)/shard_map/erd,erf->edf/dot_general | solution.py:921
  142.6 0.0 copy-done.9
  142.6 0.0 copy-start.3
  142.6 0.0 copy-start.8
  142.6 3.5 %fusion.95 = f32[2,2048,256]{2,1,0:T(8,128)} fusion(bf16[2,384,2048]{2,1,0:T(8,128)(2,1)S(1)} %bitcast.243, bf16[2,384,256]{2,1,0:T(8,128)(2,1)S(1)} %bitcast.254), kind=kOutput, calls=%fused_computation.149 | convolution fusion | flops 805306368 | bytes 7733248 | tf_op jit(solution)/shard_map/erd,erf->edf/dot_general | solution.py:922
  146.1 0.0 copy-done.3
  146.1 0.0 copy-done.8
  146.1 3.3 %fusion.96 = f32[2,256,2048]{2,1,0:T(8,128)} fusion(bf16[2,384,256]{2,1,0:T(8,128)(2,1)S(1)} %bitcast.253, bf16[2,384,2048]{2,1,0:T(8,128)(2,1)S(1)} %bitcast.248), kind=kOutput, calls=%fused_computation.150 | convolution fusion | flops 805306368 | bytes 7733248 | tf_op jit(solution)/shard_map/erf,erd->efd/dot_general | solution.py:923
  (7 shorter events, 0.1 us)
Async XLA Ops:
  124.6 4.2 %copy-start.7 = (f32[2,2,128,256]{3,2,1,0:T(8,128)S(1)}, f32[2,2,128,256]{3,2,1,0:T(8,128)}, u32[]{:S(2)}) copy-start(f32[2,2,128,256]{3,2,1,0:T(8,128)} %get-tuple-element.33) | copy-start | bytes 1572868
  124.6 4.4 %copy-start.2 = (f32[192,512]{1,0:T(8,128)S(1)}, f32[192,512]{1,0:T(8,128)}, u32[]{:S(2)}) copy-start(f32[192,512]{1,0:T(8,128)} %get-tuple-element.29) | copy-start | bytes 1179652
  124.6 4.4 %copy-start.4 = (bf16[192,512]{1,0:T(8,128)(2,1)S(1)}, bf16[192,512]{1,0:T(8,128)(2,1)}, u32[]{:S(2)}) copy-start(bf16[192,512]{1,0:T(8,128)(2,1)} %value_ref.1) | copy-start | bytes 589828
  124.6 4.7 %copy-start = (f32[192,256]{1,0:T(8,128)S(1)}, f32[192,256]{1,0:T(8,128)}, u32[]{:S(2)}) copy-start(f32[192,256]{1,0:T(8,128)} %get-tuple-element.28) | copy-start | bytes 589828
  135.2 2.5 %copy-start.5 = (bf16[8,192,512]{2,1,0:T(8,128)(2,1)S(1)}, bf16[8,192,512]{2,1,0:T(8,128)(2,1)}, u32[]{:S(2)}) copy-start(bf16[8,192,512]{2,1,0:T(8,128)(2,1)} %get-tuple-element.27) | copy-start | bytes 4718596
  135.2 2.5 %copy-start.6 = (bf16[8,192,256]{2,1,0:T(8,128)(2,1)S(1)}, bf16[8,192,256]{2,1,0:T(8,128)(2,1)}, u32[]{:S(2)}) copy-start(bf16[8,192,256]{2,1,0:T(8,128)(2,1)} %get-tuple-element.26) | copy-start | bytes 2359300
  136.0 3.2 %copy-start.1 = (bf16[2,8,48,2048]{3,2,1,0:T(8,128)(2,1)S(1)}, bf16[2,8,48,2048]{3,2,1,0:T(8,128)(2,1)}, u32[]{:S(2)}) copy-start(bf16[2,8,48,2048]{3,2,1,0:T(8,128)(2,1)} %get-tuple-element.21) | copy-start | bytes 9437188
  136.0 3.1 %copy-start.10 = (bf16[2,8,48,256]{3,2,1,0:T(8,128)(2,1)S(1)}, bf16[2,8,48,256]{3,2,1,0:T(8,128)(2,1)}, u32[]{:S(2)}) copy-start(bf16[2,8,48,256]{3,2,1,0:T(8,128)(2,1)} %get-tuple-element.22) | copy-start | bytes 1179652
  139.1 3.5 %copy-start.9 = (bf16[2,8,48,256]{3,2,1,0:T(8,128)(2,1)S(1)}, bf16[2,8,48,256]{3,2,1,0:T(8,128)(2,1)}, u32[]{:S(2)}) copy-start(bf16[2,8,48,256]{3,2,1,0:T(8,128)(2,1)} %get-tuple-element.23) | copy-start | bytes 1179652
  142.6 3.5 %copy-start.3 = (bf16[2,8,48,2048]{3,2,1,0:T(8,128)(2,1)S(1)}, bf16[2,8,48,2048]{3,2,1,0:T(8,128)(2,1)}, u32[]{:S(2)}) copy-start(bf16[2,8,48,2048]{3,2,1,0:T(8,128)(2,1)} %get-tuple-element.25) | copy-start | bytes 9437188
  142.6 3.5 %copy-start.8 = (bf16[2,8,48,256]{3,2,1,0:T(8,128)(2,1)S(1)}, bf16[2,8,48,256]{3,2,1,0:T(8,128)(2,1)}, u32[]{:S(2)}) copy-start(bf16[2,8,48,256]{3,2,1,0:T(8,128)(2,1)} %get-tuple-element.24) | copy-start | bytes 1179652
